TPU v7x, 128 devices: a whole 4x4x4 slice. The times are simulated.
128 devices in a mesh: rep: 2 (over z_hi), fs: 32 (over z_lo, y, x), tp: 2 (over core).
Axes of the slice: x: 4, y: 4, z: 4 (z_hi: 2, z_lo: 2; z = z_hi * 2 + z_lo), core: 2. Of those that a mesh axis runs over, the one named last changes fastest.
Arguments:
- stream_in: bfloat16 [64, 1024, 2048], P(('rep', 'fs'), None, 'tp'), may hold values from -48 to 48
- decay_shift: float32 [64, 1024], P(('rep', 'fs')), may hold values from -1.5 to 0, as said below
- mixer_gain: float32 [2048], replicated, may hold values from 0.1 to 1.9
- gate_weight: bfloat16 [2048, 1024], P('fs', 'tp'), may hold values from -0.125 to 0.125
- input_weight: bfloat16 [2048, 1024], P('fs', 'tp'), may hold values from -0.125 to 0.125
- filter_taps: float32 [4, 1024], P(None, 'tp'), may hold values from -3 to 3
- recur_gate: bfloat16 [4, 256, 256], P('tp'), may hold values from -0.375 to 0.375
- inlet_gate: bfloat16 [4, 256, 256], P('tp'), may hold values from -0.375 to 0.375
- decay_param: float32 [1024], P('tp'), may hold values from 1.5 to 12
- mixer_out: bfloat16 [1024, 2048], P('tp', 'fs'), may hold values from -0.1875 to 0.1875
- feedforward_gain: float32 [2048], replicated, may hold values from 0.1 to 1.9
- up_weight: bfloat16 [2048, 4096], P('fs', 'tp'), may hold values from -0.125 to 0.125
- down_weight: bfloat16 [4096, 2048], P('tp', 'fs'), may hold values from -0.09375 to 0.09375
- final_gain: float32 [2048], P('tp'), may hold values from 0.1 to 1.9
Outputs:
- layer_out: bfloat16 [64, 1024, 2048], P(('rep', 'fs'), None, 'tp')
Inputs may be any that keep to these rules, and one draw needn't show every extreme that they name: `decay_shift`: every entry is negative.
All inputs are finite; a program needn't handle non-finite values.
Results may differ from a plain program's by a relative error of at most 0.015.
Values may be sent and summed in bfloat16 or wider, within the bound.
No kernel may reach another device: no remote copies, remote signals or barrier semaphores. Data moves between devices by JAX's collectives and lax.ppermute only.
A program may use at most 128 MiB of HBM per device.

v0:
```python
import jax
import jax.numpy as jnp
from jax import lax
from jax.sharding import PartitionSpec as P

D = 2048
epsilon = 1e-06
rate_scale = 8.0


def rows_first(arrays, axis, dims):
    turned = [jnp.moveaxis(a, dim, 0) for a, dim in zip(arrays, dims)]
    widths = [t[0].size for t in turned]
    both = jnp.concatenate([t.reshape(-1, w) for t, w in zip(turned, widths)], axis=1)
    out = lax.all_gather(both, axis, axis=0, tiled=True)
    parts = jnp.split(out, [sum(widths[:k]) for k in range(1, len(widths))], axis=1)
    return tuple(
        (
            jnp.moveaxis(b.reshape(-1, *t.shape[1:]), 0, dim)
            for b, t, dim in zip(parts, turned, dims)
        )
    )


def side_by_side(arrays, axis, dim, along):
    ends, at = ([], 0)
    for a in arrays[:-1]:
        at += a.shape[along]
        ends.append(at)
    both = jnp.concatenate(arrays, axis=along)
    return tuple(jnp.split(lax.all_gather(both, axis, axis=dim, tiled=True), ends, axis=along))


def cut_along(x, dim, size):
    before, after = (x.shape[:dim], x.shape[dim + 1 :])
    return jnp.moveaxis(x.reshape(*before, size, -1, *after), dim, 0)


def summed_on_arrival(x, axis, dim):
    parts = cut_along(x, dim, lax.axis_size(axis))
    arrived = lax.all_to_all(parts, axis, split_axis=0, concat_axis=0, tiled=True)
    return arrived.astype(jnp.float32).sum(axis=0)


def from_everyone(x, axis):
    copies = jnp.broadcast_to(x, (lax.axis_size(axis), *x.shape))
    return lax.all_to_all(copies, axis, split_axis=0, concat_axis=0, tiled=True)


def over_copies(x, axis):
    return from_everyone(x, axis).sum(axis=0)


def norm_rows(values, row_gain):
    mean_sq = jnp.mean(values * values, axis=-1, keepdims=True)
    return values * lax.rsqrt(mean_sq + epsilon) * row_gain


def combine(earlier, later):
    return (earlier[0] * later[0], later[0] * earlier[1] + later[1])


def local(
    stream_in,
    decay_shift,
    mixer_gain,
    gate_weight,
    input_weight,
    filter_taps,
    recur_gate,
    inlet_gate,
    decay_param,
    mixer_out,
    feedforward_gain,
    up_weight,
    down_weight,
    final_gain,
):
    num_seq, length, half_width = stream_in.shape
    up_whole, complete_contraction = rows_first((up_weight, down_weight), "fs", (0, 1))
    whole = lax.all_gather(stream_in, "tp", axis=2, tiled=True)
    flat_rows = num_seq * length
    normed = norm_rows(whole.reshape(flat_rows, -1).astype(jnp.float32), mixer_gain).astype(
        jnp.bfloat16
    )
    channels = gate_weight.shape[1]
    fragments = side_by_side((gate_weight, input_weight), "fs", 0, 1)
    gate_logits = jnp.dot(normed, fragments[0], preferred_element_type=jnp.float32)
    input_pre = jnp.dot(normed, fragments[1], preferred_element_type=jnp.float32)
    gate_logits = gate_logits.astype(jnp.bfloat16)
    input_pre = input_pre.astype(jnp.bfloat16)
    branch = jax.nn.gelu(gate_logits.astype(jnp.float32), approximate=True)
    num_taps = filter_taps.shape[0]
    extended_front = jnp.pad(
        input_pre.astype(jnp.float32).reshape(num_seq, length, channels),
        ((0, 0), (num_taps - 1, 0), (0, 0)),
    )
    filtered = jnp.zeros((num_seq, length, channels), jnp.float32)
    for offset in range(num_taps):
        filtered = (
            filtered
            + extended_front[:, offset : offset + length] * filter_taps[offset][None, None, :]
        )
    filtered = filtered.astype(jnp.bfloat16).reshape(flat_rows, channels)
    num_blocks = recur_gate.shape[0]
    grouped = filtered.reshape(flat_rows, num_blocks, recur_gate.shape[1])
    recur = jax.nn.sigmoid(
        jnp.einsum("lni,nij->lnj", grouped, recur_gate, preferred_element_type=jnp.float32).reshape(
            flat_rows, channels
        )
    )
    inlet = jax.nn.sigmoid(
        jnp.einsum("lni,nij->lnj", grouped, inlet_gate, preferred_element_type=jnp.float32).reshape(
            flat_rows, channels
        )
    )
    logarithm_decay = (
        -rate_scale * recur * jax.nn.softplus(-decay_param)[None, :]
        + decay_shift.reshape(flat_rows)[:, None]
    )
    decay = jnp.exp(logarithm_decay).reshape(num_seq, length, channels)
    drive = (
        jnp.sqrt(-jnp.expm1(2.0 * logarithm_decay)) * inlet * filtered.astype(jnp.float32)
    ).reshape(num_seq, length, channels)
    states = lax.associative_scan(combine, (decay, drive), axis=1)[1]
    mixed = (states.reshape(flat_rows, channels) * branch).astype(jnp.bfloat16)
    mixer_terms = (
        jnp.dot(
            mixed,
            lax.all_gather(mixer_out, "fs", axis=1, tiled=True),
            preferred_element_type=jnp.float32,
        )
        .astype(jnp.bfloat16)
        .astype(jnp.float32)
    )
    mixer_sum = summed_on_arrival(mixer_terms.astype(jnp.bfloat16), "tp", 1)
    stream_mid = (stream_in.reshape(flat_rows, half_width).astype(jnp.float32) + mixer_sum).astype(
        jnp.bfloat16
    )
    stream_whole = lax.all_gather(stream_mid, "tp", axis=1, tiled=True)
    normed_mid = norm_rows(stream_whole.astype(jnp.float32), feedforward_gain).astype(jnp.bfloat16)
    up_proj = jnp.dot(normed_mid, up_whole, preferred_element_type=jnp.float32)
    activated = jnp.square(jax.nn.relu(up_proj)).astype(jnp.bfloat16)
    ffn_terms = (
        jnp.dot(activated, complete_contraction, preferred_element_type=jnp.float32)
        .astype(jnp.bfloat16)
        .astype(jnp.float32)
    )
    ffn_sum = summed_on_arrival(ffn_terms.astype(jnp.bfloat16), "tp", 1)
    total = stream_mid.astype(jnp.float32) + ffn_sum
    squares_sum = over_copies(jnp.sum(total * total, axis=1), "tp")
    layer_out = total * lax.rsqrt(squares_sum / D + epsilon)[:, None] * final_gain[None, :]
    return layer_out.astype(jnp.bfloat16).reshape(num_seq, length, half_width)


def solution(mesh):
    return jax.shard_map(
        local,
        mesh=mesh,
        in_specs=(
            P(("rep", "fs"), None, "tp"),
            P(("rep", "fs"), None),
            P(),
            P("fs", "tp"),
            P("fs", "tp"),
            P(None, "tp"),
            P("tp", None, None),
            P("tp", None, None),
            P("tp"),
            P("tp", "fs"),
            P(),
            P("fs", "tp"),
            P("tp", "fs"),
            P("tp"),
        ),
        out_specs=P(("rep", "fs"), None, "tp"),
        check_vma=False,
    )
```

profile of v0, /device:TPU:1, one launch (start us, length us, event | category | flops | bytes accessed | tf_op | source)
XLA Modules:
  0.0 648.5 jit_solution(12053179371689697069)
XLA Ops:
  11.2 17.8 %all-gather.6.cloned.1.call-done = bf16[1,1024,2048]{2,1,0:T(8,128)(2,1)} async-done(((bf16[1,1024,1024]{2,1,0:T(8,128)(2,1)}), bf16[1,1024,2048]{2,1,0:T(8,128)(2,1)}) %all-gather.6.cloned.1.call-update) | async-done | bytes 4194320 | tf_op jit(solution)/shard_map/all_gather | solution.py:81
  29.0 3.1 fusion.3
  32.1 135.9 %all-gather.8.cloned.1.call-done = bf16[2048,1024]{1,0:T(8,128)(2,1)} async-done(((bf16[64,1024]{1,0:T(8,128)(2,1)}), bf16[2048,1024]{1,0:T(8,128)(2,1)}) %all-gather.8.cloned.1.call-update) | async-done | bytes 4194320 | tf_op jit(solution)/shard_map/all_gather | solution.py:31
  168.0 5.2 fusion.39
  175.9 2.0 add_divide_fusion.1
  177.9 1.8 copy.48
  179.7 2.0 add_divide_fusion
  181.7 1.9 copy.49
  183.6 5.2 fusion.38
  188.8 3.5 slice.263
  192.2 3.5 slice.264
  195.7 6.3 slice.262
  202.0 6.3 slice.266
  208.2 3.7 fusion.83
  211.9 2.1 slice.269
  214.0 2.1 slice.270
  216.0 3.6 slice.268
  219.7 3.6 slice.272
  223.3 2.7 fusion.84
  226.0 2.5 slice.275
  228.5 2.5 slice.276
  231.0 2.5 slice.274
  233.5 2.5 slice.278
  236.0 2.0 fusion.85
  242.5 1.8 fusion.86
  289.9 2.5 slice.273
  292.4 2.5 slice.330
  296.2 3.7 slice.267
  299.9 2.1 slice.332
  303.5 6.3 slice.261
  318.2 2.1 pad.83
  321.5 8.7 %pad.85 = f32[1,1024,512]{2,1,0:T(8,128)} pad(f32[1,512,512]{2,1,0:T(8,128)} %add.272, f32[]{:T(128)} %constant.10.clone.1), padding=0_0_0x1_0_1x0_0_0 | pad | bytes 3145732 | tf_op jit(solution)/shard_map/pad | solution.py:125
  330.2 1.7 fusion.52
  332.1 4.7 pad.84
  336.8 11.0 %convolution_convert_fusion = bf16[1024,2048]{1,0:T(8,128)(2,1)} fusion(bf16[512,2048]{0,1:T(8,128)(2,1)} %all-gather.10.cloned.1.call-done, f32[1,1024,512]{2,1,0:T(8,128)} %pad.84, f32[1,1024,512]{2,1,0:T(8,128)S(1)} %copy-done.8, bf16[2048,1024]{1,0:T(8,128)(2,1)} %all-gather.8.cloned.1.call-done, ...), kind=kOutput, calls=%fused_computation.32 | convolution fusion | flops 4312268800 | bytes 16789504 | tf_op jit(solution)/shard_map/dot_general | solution.py:128
  347.8 2.6 copy.60
  350.5 27.4 %all_to_all.16 = bf16[2,1024,1024]{2,1,0:T(8,128)(2,1)S(1)} all-to-all(bf16[2,1024,1024]{2,1,0:T(8,128)(2,1)S(1)} %bitcast.68), channel_id=1, replica_groups=mesh['rep'=2,'fs'=32,'tp'=2] {'tp'}, dimensions={0} | all-to-all | bytes 8388608 | tf_op jit(solution)/shard_map/all_to_all | solution.py:41
  378.9 2.0 copy-done.2
  380.9 2.2 fusion.14
  384.1 16.1 %all-gather.12.cloned.1.call-done = bf16[1024,2048]{1,0:T(8,128)(2,1)} async-done(((bf16[1024,1024]{1,0:T(8,128)(2,1)}), bf16[1024,2048]{1,0:T(8,128)(2,1)}) %all-gather.12.cloned.1.call-update) | async-done | bytes 4194320 | tf_op jit(solution)/shard_map/all_gather | solution.py:140
  400.2 3.1 fusion
  403.3 189.5 %all-gather.14.cloned.1.call-done = bf16[2048,4096]{1,0:T(8,128)(2,1)} async-done(((bf16[64,4096]{1,0:T(8,128)(2,1)}), bf16[2048,4096]{1,0:T(8,128)(2,1)}) %all-gather.14.cloned.1.call-update) | async-done | bytes 16777232 | tf_op jit(solution)/shard_map/all_gather | solution.py:15
  592.9 25.7 %fusion.21 = bf16[1024,2048]{1,0:T(8,128)(2,1)} fusion(bf16[2048,4096]{1,0:T(8,128)(2,1)} %all-gather.14.cloned.1.call-done, bf16[1024,2048]{1,0:T(8,128)(2,1)} %all-gather.12.cloned.1.call-done, f32[2048]{0:T(1024)S(1)} %copy-done.33, f32[1024]{0:T(1024)S(1)} %add_rsqrt_fusion.1), kind=kOutput, calls=%fused_computation.31 | convolution fusion | flops 17196646400 | bytes 25178112 | tf_op jit(solution)/shard_map/dot_general | solution.py:145
  618.5 2.6 copy.59
  621.2 7.8 %all_to_all.17 = bf16[2,1024,1024]{2,1,0:T(8,128)(2,1)S(1)} all-to-all(bf16[2,1024,1024]{2,1,0:T(8,128)(2,1)S(1)} %bitcast.69), channel_id=1, replica_groups=mesh['rep'=2,'fs'=32,'tp'=2] {'tp'}, dimensions={0} | all-to-all | bytes 8388608 | tf_op jit(solution)/shard_map/all_to_all | solution.py:41
  630.0 2.0 copy-done.3
  632.6 3.7 all_to_all.18
  636.4 5.6 fusion.18
  (182 shorter events, 73.2 us)
Async XLA Ops:
  6.5 169.3 %copy-start = (bf16[2,256,256]{2,1,0:T(8,128)(2,1)S(1)}, bf16[2,256,256]{2,1,0:T(8,128)(2,1)}, u32[]{:S(2)}) copy-start(bf16[2,256,256]{2,1,0:T(8,128)(2,1)} %param.20) | copy-start | bytes 786436
  6.5 161.5 %copy-start.31 = (f32[2048]{0:T(1024)S(1)}, f32[2048]{0:T(1024)}, u32[]{:S(2)}) copy-start(f32[2048]{0:T(1024)} %param.16) | copy-start | bytes 24580
  6.5 22.5 %all-gather.6.cloned.1.call-start = ((), (), s32[]{:S(2)}) async-start(), calls=%async_computation.3 | async-start | bytes 6291456 | tf_op jit(solution)/shard_map/all_gather | solution.py:81
  7.3 160.7 %all-gather.8.cloned.1.call-start = ((), (), s32[]{:S(2)}) async-start(), calls=%async_computation.4 | async-start | bytes 4325376 | tf_op jit(solution)/shard_map/all_gather | solution.py:31
  8.9 327.9 %all-gather.10.cloned.1.call-start = ((), (), s32[]{:S(2)}) async-start(), calls=%async_computation.5 | async-start | bytes 2162688 | tf_op jit(solution)/shard_map/all_gather | solution.py:130
  9.6 390.6 %all-gather.12.cloned.1.call-start = ((), (), s32[]{:S(2)}) async-start(), calls=%async_computation.6 | async-start | bytes 6291456 | tf_op jit(solution)/shard_map/all_gather | solution.py:140
  32.1 141.1 %copy-start.28 = (f32[1024]{0:T(1024)}, f32[1024]{0:T(1024)S(1)}, u32[]{:S(2)}) copy-start(f32[1024]{0:T(1024)S(1)} %add_rsqrt_fusion.2) | copy-start | bytes 12292
  177.9 1.8 copy-start.30
  181.7 1.9 copy-start.26
  289.8 20.6 %copy-start.17 = (f32[1,2,512]{2,1,0:T(2,128)S(1)}, f32[1,2,512]{2,1,0:T(2,128)}, u32[]{:S(2)}) copy-start(f32[1,2,512]{2,1,0:T(2,128)} %slice.310) | copy-start | bytes 12292
  289.8 20.6 %copy-start.18 = (f32[1,2,512]{2,1,0:T(2,128)S(1)}, f32[1,2,512]{2,1,0:T(2,128)}, u32[]{:S(2)}) copy-start(f32[1,2,512]{2,1,0:T(2,128)} %slice.311) | copy-start | bytes 12292
  289.8 20.6 %copy-start.19 = (f32[1,2,512]{2,1,0:T(2,128)S(1)}, f32[1,2,512]{2,1,0:T(2,128)}, u32[]{:S(2)}) copy-start(f32[1,2,512]{2,1,0:T(2,128)} %slice.312) | copy-start | bytes 12292
  289.8 20.6 %copy-start.20 = (f32[1,2,512]{2,1,0:T(2,128)S(1)}, f32[1,2,512]{2,1,0:T(2,128)}, u32[]{:S(2)}) copy-start(f32[1,2,512]{2,1,0:T(2,128)} %slice.314) | copy-start | bytes 12292
  289.8 20.6 %copy-start.14 = (f32[1,4,512]{2,1,0:T(4,128)S(1)}, f32[1,4,512]{2,1,0:T(4,128)}, u32[]{:S(2)}) copy-start(f32[1,4,512]{2,1,0:T(4,128)} %get-tuple-element.24) | copy-start | bytes 24580
  289.8 21.4 %copy-start.15 = (f32[1,3,512]{2,1,0:T(4,128)S(1)}, f32[1,3,512]{2,1,0:T(4,128)}, u32[]{:S(2)}) copy-start(f32[1,3,512]{2,1,0:T(4,128)} %slice.303) | copy-start | bytes 18436
  289.8 21.4 %copy-start.16 = (f32[1,3,512]{2,1,0:T(4,128)S(1)}, f32[1,3,512]{2,1,0:T(4,128)}, u32[]{:S(2)}) copy-start(f32[1,3,512]{2,1,0:T(4,128)} %slice.320) | copy-start | bytes 18436
  289.8 21.4 %copy-start.25 = (f32[1,1,512]{2,1,0:T(1,128)S(1)}, f32[1,1,512]{2,1,0:T(1,128)}, u32[]{:S(2)}) copy-start(f32[1,1,512]{2,1,0:T(1,128)} %slice.342) | copy-start | bytes 6148
  289.8 21.5 %copy-start.13 = (f32[1,7,512]{2,1,0:T(8,128)S(1)}, f32[1,7,512]{2,1,0:T(8,128)}, u32[]{:S(2)}) copy-start(f32[1,7,512]{2,1,0:T(8,128)} %slice.322) | copy-start | bytes 43012
  289.9 21.5 %copy-start.24 = (f32[1,1,512]{2,1,0:T(1,128)S(1)}, f32[1,1,512]{2,1,0:T(1,128)}, u32[]{:S(2)}) copy-start(f32[1,1,512]{2,1,0:T(1,128)} %slice.341) | copy-start | bytes 6148
  289.9 21.6 %copy-start.11 = (f32[1,15,512]{2,1,0:T(8,128)S(1)}, f32[1,15,512]{2,1,0:T(8,128)}, u32[]{:S(2)}) copy-start(f32[1,15,512]{2,1,0:T(8,128)} %slice.291) | copy-start | bytes 92164
  289.9 21.6 %copy-start.12 = (f32[1,15,512]{2,1,0:T(8,128)S(1)}, f32[1,15,512]{2,1,0:T(8,128)}, u32[]{:S(2)}) copy-start(f32[1,15,512]{2,1,0:T(8,128)} %slice.324) | copy-start | bytes 92164
  289.9 21.6 %copy-start.23 = (f32[1,1,512]{2,1,0:T(1,128)S(1)}, f32[1,1,512]{2,1,0:T(1,128)}, u32[]{:S(2)}) copy-start(f32[1,1,512]{2,1,0:T(1,128)} %slice.340) | copy-start | bytes 6148
  311.6 6.2 copy-start.6
  311.6 6.2 copy-start.7
  314.9 3.1 copy-start.22
  321.5 10.4 %copy-start.21 = (f32[1,1,512]{2,1,0:T(1,128)S(1)}, f32[1,1,512]{2,1,0:T(1,128)}, u32[]{:S(2)}) copy-start(f32[1,1,512]{2,1,0:T(1,128)} %slice.335) | copy-start | bytes 6148
  330.2 6.6 %copy-start.29 = (f32[1024]{0:T(1024)S(1)}, f32[1024]{0:T(1024)}, u32[]{:S(2)}) copy-start(f32[1024]{0:T(1024)} %copy-done.28) | copy-start | bytes 12292
  330.2 6.6 %copy-start.32 = (f32[2048]{0:T(1024)S(1)}, f32[2048]{0:T(1024)}, u32[]{:S(2)}) copy-start(f32[2048]{0:T(1024)} %param.16) | copy-start | bytes 24580
  331.9 4.9 copy-start.8
  377.9 3.0 copy-start.4
  378.9 2.0 copy-start.2
  380.9 2.3 copy-start.9
  380.9 2.3 copy-start.10
  383.1 209.7 %copy-start.33 = (f32[2048]{0:T(1024)S(1)}, f32[2048]{0:T(1024)}, u32[]{:S(2)}) copy-start(f32[2048]{0:T(1024)} %param.24) | copy-start | bytes 24580
  383.1 209.7 %all-gather.14.cloned.1.call-start = ((), (), s32[]{:S(2)}) async-start(), calls=%async_computation.7 | async-start | bytes 17301504 | tf_op jit(solution)/shard_map/all_gather | solution.py:15
  628.9 3.0 copy-start.5
  630.0 2.0 copy-start.3
  632.0 4.4 copy-start.27
  636.4 5.6 copy-start.1
Sparse Core Ops, SparseCore 0:
  9.0 19.9 all-gather.5
  30.7 137.2 all-gather.7
  169.6 151.5 all-gather.9
  383.3 16.9 all-gather.11
  401.7 191.0 all-gather.13
where the time goes:
time: 652 us; the launch traced here: 649 us
  waiting for transfers between devices  361 us (55%)
  local copies, waits for them, and re-layouts  137 us (21%)
  other arithmetic  52.2 us (8%)
  matrix products  45.9 us (7%)
  blocking collectives  38.9 us (6%)
  between operations  13.8 us (2%)
    all_gather x1, waiting for transfers between devices, rows_first(): out = lax.all_gather(both, axis, axis=0, tiled=True)  190 us
    all_gather x1, waiting for transfers between devices, side_by_side(): lax.all_gather(both, axis, axis=dim, tiled=True)  136 us
    slice x60, local copies, waits for them, and re-layouts, local(): states = lax.associative_scan(combine, (decay, drive), axis=1)[1]  106 us
    all_to_all x2, blocking collectives, summed_on_arrival(): lax.all_to_all(parts, axis, split_axis=0, concat_axis=0, tiled=True)  35.2 us
    dot_general x1, matrix products, local(): jnp.dot(activated, complete_contraction, preferred_element_type=jnp.float32)  25.7 us
    all_gather x1, waiting for transfers between devices, local(): whole = lax.all_gather(stream_in, 'tp', axis=2, tiled=True)  17.8 us
    all_gather x1, waiting for transfers between devices, local(): stream_whole = lax.all_gather(stream_mid, 'tp', axis=1, tiled=True)  16.1 us
    pad x18, local copies, waits for them, and re-layouts, local(): states = lax.associative_scan(combine, (decay, drive), axis=1)[1]  16 us
  transfers between devices with their start and end apart: 5, of which 4 were waited for; matrix products, arithmetic and copies ran while one was open for 27% of the time, Pallas kernels for 0%

commit v1 on v0

--- a/solution.py
+++ b/solution.py
@@ -12,7 +12,9 @@
     turned = [jnp.moveaxis(a, dim, 0) for a, dim in zip(arrays, dims)]
     widths = [t[0].size for t in turned]
     both = jnp.concatenate([t.reshape(-1, w) for t, w in zip(turned, widths)], axis=1)
-    out = lax.all_gather(both, axis, axis=0, tiled=True)
+    out = jnp.concatenate(
+        lax.all_to_all(jnp.stack([both] * lax.axis_size(axis)), axis, 0, 0), axis=0
+    )
     parts = jnp.split(out, [sum(widths[:k]) for k in range(1, len(widths))], axis=1)
     return tuple(
         (

time: 652 us -> 744 us (1.14)
  the two profiles are of different devices: /device:TPU:1 before, /device:TPU:35 now
where the time goes in v1:
time: 744 us; the launch traced here: 740 us
  waiting for transfers between devices  435 us (58%)
  local copies, waits for them, and re-layouts  136 us (18%)
  other arithmetic  60.8 us (8%)
  matrix products  45.8 us (6%)
  blocking collectives  41.2 us (6%)
  between operations  13.6 us (2%)
  starting transfers between devices  8.24 us (1%)
    all_to_all x1, waiting for transfers between devices, rows_first(): lax.all_to_all(jnp.stack([both] * lax.axis_size(axis)), axis, 0, 0)  266 us
    all_gather x1, waiting for transfers between devices, side_by_side(): lax.all_gather(both, axis, axis=dim, tiled=True)  134 us
    slice x60, local copies, waits for them, and re-layouts, local(): states = lax.associative_scan(combine, (decay, drive), axis=1)[1]  107 us
    all_to_all x2, blocking collectives, summed_on_arrival(): lax.all_to_all(parts, axis, split_axis=0, concat_axis=0, tiled=True)  37.4 us
    dot_general x1, matrix products, local(): jnp.dot(activated, complete_contraction, preferred_element_type=jnp.float32)  25.6 us
    all_gather x1, waiting for transfers between devices, local(): stream_whole = lax.all_gather(stream_mid, 'tp', axis=1, tiled=True)  18.4 us
    mul x8, other arithmetic, combine(): return (earlier[0] * later[0], later[0] * earlier[1] + later[1])  15.9 us
  transfers between devices with their start and end apart: 5, of which 4 were waited for; matrix products, arithmetic and copies ran while one was open for 25% of the time, Pallas kernels for 0%

profile of v1, /device:TPU:35, one launch (start us, length us, event | category | flops | bytes accessed | tf_op | source)
XLA Modules:
  0.0 739.9 jit_solution(16734933471744537306)
XLA Ops:
  13.0 14.9 %all-gather.5.cloned.1.call-done = bf16[1,1024,2048]{2,1,0:T(8,128)(2,1)} async-done(((bf16[1,1024,1024]{2,1,0:T(8,128)(2,1)}), bf16[1,1024,2048]{2,1,0:T(8,128)(2,1)}) %all-gather.5.cloned.1.call-update) | async-done | bytes 4194320 | tf_op jit(solution)/shard_map/all_gather | solution.py:83
  27.9 3.1 fusion.3
  31.0 133.9 %all-gather.7.cloned.1.call-done = bf16[2048,1024]{1,0:T(8,128)(2,1)} async-done(((bf16[64,1024]{1,0:T(8,128)(2,1)}), bf16[2048,1024]{1,0:T(8,128)(2,1)}) %all-gather.7.cloned.1.call-update) | async-done | bytes 4194320 | tf_op jit(solution)/shard_map/all_gather | solution.py:33
  164.9 5.2 fusion.39
  172.9 2.0 add_divide_fusion.1
  176.7 2.0 add_divide_fusion
  178.7 1.9 copy.49
  180.6 5.2 fusion.38
  185.8 6.3 slice.261
  192.2 6.2 slice.266
  198.4 6.2 slice.262
  204.6 3.6 slice.334
  208.2 3.5 slice.264
  211.7 3.5 slice.263
  215.2 3.7 fusion.83
  218.9 3.6 slice.272
  222.5 3.6 slice.268
  226.2 2.0 slice.270
  228.2 2.1 slice.269
  230.3 2.7 fusion.84
  233.0 2.5 slice.273
  235.6 2.5 slice.278
  238.0 2.5 slice.274
  240.5 2.5 slice.330
  243.0 2.5 slice.276
  245.5 2.5 slice.275
  248.0 2.0 fusion.85
  302.7 2.1 slice.332
  304.8 3.7 slice.267
  320.8 2.1 pad.82
  326.0 4.7 pad.84
  331.1 11.0 %convolution_convert_fusion = bf16[1024,2048]{1,0:T(8,128)(2,1)} fusion(bf16[512,2048]{0,1:T(8,128)(2,1)} %all-gather.9.cloned.1.call-done, f32[1,1024,512]{2,1,0:T(8,128)} %pad.84, f32[1,1024,512]{2,1,0:T(8,128)S(1)} %pad.85, bf16[2048,1024]{1,0:T(8,128)(2,1)} %all-gather.7.cloned.1.call-done, bf16[1,1024,2048]{2,1,0:T(8,128)(2,1)} %all-gather.5.cloned.1.call-done, ...), kind=kOutput, calls=%fused_computation.32 | convolution fusion | flops 4312268800 | bytes 16789504 | tf_op jit(solution)/shard_map/dot_general | solution.py:130
  342.1 2.6 copy.60
  344.7 29.2 %all_to_all.21 = bf16[2,1024,1024]{2,1,0:T(8,128)(2,1)} all-to-all(bf16[2,1024,1024]{2,1,0:T(8,128)(2,1)S(1)} %bitcast.69), channel_id=1, replica_groups=mesh['rep'=2,'fs'=32,'tp'=2] {'tp'}, dimensions={0} | all-to-all | bytes 8388608 | tf_op jit(solution)/shard_map/all_to_all | solution.py:43
  373.9 5.9 stack.2
  379.8 8.1 %all-to-all-start.1 = ((bf16[32,64,4096]{2,1,0:T(8,128)(2,1)}), bf16[32,64,4096]{2,1,0:T(8,128)(2,1)}, u32[]{:S(2)}, u32[]{:S(2)}) async-start(bf16[32,64,4096]{2,1,0:T(8,128)(2,1)} %stack.2), calls=%async_computation.1 | async-start | bytes 33554432 | tf_op jit(solution)/shard_map/all_to_all | solution.py:16
  388.0 4.0 convert_reduce_fusion.1
  392.0 2.1 copy-done.2
  394.0 2.2 fusion.14
  396.3 18.4 %all-gather.11.cloned.1.call-done = bf16[1024,2048]{1,0:T(8,128)(2,1)} async-done(((bf16[1024,1024]{1,0:T(8,128)(2,1)}), bf16[1024,2048]{1,0:T(8,128)(2,1)}) %all-gather.11.cloned.1.call-update) | async-done | bytes 4194320 | tf_op jit(solution)/shard_map/all_gather | solution.py:142
  414.6 3.1 fusion
  417.7 266.1 %all-to-all-done.1 = bf16[32,64,4096]{2,1,0:T(8,128)(2,1)} async-done(((bf16[32,64,4096]{2,1,0:T(8,128)(2,1)}), bf16[32,64,4096]{2,1,0:T(8,128)(2,1)}, u32[]{:S(2)}, u32[]{:S(2)}) %all-to-all-start.1) | async-done | bytes 16777248 | tf_op jit(solution)/shard_map/all_to_all | solution.py:16
  683.8 25.6 %fusion.21 = bf16[1024,2048]{1,0:T(8,128)(2,1)} fusion(bf16[2048,4096]{1,0:T(8,128)(2,1)} %bitcast.18, bf16[1024,2048]{1,0:T(8,128)(2,1)} %all-gather.11.cloned.1.call-done, f32[2048]{0:T(1024)S(1)} %copy-done.18, f32[1024]{0:T(1024)S(1)} %add_rsqrt_fusion.1), kind=kOutput, calls=%fused_computation.31 | convolution fusion | flops 17196646400 | bytes 25178112 | tf_op jit(solution)/shard_map/dot_general | solution.py:147
  709.4 2.6 copy.59
  712.1 8.2 %all_to_all.22 = bf16[2,1024,1024]{2,1,0:T(8,128)(2,1)S(1)} all-to-all(bf16[2,1024,1024]{2,1,0:T(8,128)(2,1)S(1)} %bitcast.70), channel_id=1, replica_groups=mesh['rep'=2,'fs'=32,'tp'=2] {'tp'}, dimensions={0} | all-to-all | bytes 8388608 | tf_op jit(solution)/shard_map/all_to_all | solution.py:43
  721.4 1.9 copy-done.3
  724.0 3.7 all_to_all.23
  727.8 5.6 fusion.18
  (152 shorter events, 81.0 us)
Async XLA Ops:
  6.5 166.3 %copy-start = (bf16[2,256,256]{2,1,0:T(8,128)(2,1)S(1)}, bf16[2,256,256]{2,1,0:T(8,128)(2,1)}, u32[]{:S(2)}) copy-start(bf16[2,256,256]{2,1,0:T(8,128)(2,1)} %param.20) | copy-start | bytes 786436
  6.5 158.4 %copy-start.16 = (f32[2048]{0:T(1024)S(1)}, f32[2048]{0:T(1024)}, u32[]{:S(2)}) copy-start(f32[2048]{0:T(1024)} %param.16) | copy-start | bytes 24580
  6.5 21.4 %all-gather.5.cloned.1.call-start = ((), (), s32[]{:S(2)}) async-start(), calls=%async_computation.4 | async-start | bytes 6291456 | tf_op jit(solution)/shard_map/all_gather | solution.py:83
  7.3 157.6 %all-gather.7.cloned.1.call-start = ((), (), s32[]{:S(2)}) async-start(), calls=%async_computation.5 | async-start | bytes 4325376 | tf_op jit(solution)/shard_map/all_gather | solution.py:33
  8.9 322.2 %all-gather.9.cloned.1.call-start = ((), (), s32[]{:S(2)}) async-start(), calls=%async_computation.6 | async-start | bytes 2162688 | tf_op jit(solution)/shard_map/all_gather | solution.py:132
  31.0 139.2 %copy-start.13 = (f32[1024]{0:T(1024)}, f32[1024]{0:T(1024)S(1)}, u32[]{:S(2)}) copy-start(f32[1024]{0:T(1024)S(1)} %add_rsqrt_fusion.2) | copy-start | bytes 12292
  174.9 1.8 copy-start.15
  178.7 1.9 copy-start.11
  308.5 9.5 %copy-start.9 = (f32[1,127,512]{2,1,0:T(8,128)S(1)}, f32[1,127,512]{2,1,0:T(8,128)}, u32[]{:S(2)}) copy-start(f32[1,127,512]{2,1,0:T(8,128)} %slice.273) | copy-start | bytes 780292
  308.5 9.5 %copy-start.10 = (f32[1,127,512]{2,1,0:T(8,128)S(1)}, f32[1,127,512]{2,1,0:T(8,128)}, u32[]{:S(2)}) copy-start(f32[1,127,512]{2,1,0:T(8,128)} %slice.330) | copy-start | bytes 780292
  318.5 5.7 copy-start.6
  325.9 4.9 copy-start.7
  325.9 5.2 copy-start.14
  325.9 5.2 copy-start.17
  344.7 29.2 %copy-start.8 = (bf16[64,4096]{1,0:T(8,128)(2,1)S(1)}, bf16[64,4096]{1,0:T(8,128)(2,1)}, u32[]{:S(2)}) copy-start(bf16[64,4096]{1,0:T(8,128)(2,1)} %pad_maximum_fusion.2) | copy-start | bytes 1572868
  379.8 304.0 %all-to-all-start.1 = ((bf16[32,64,4096]{2,1,0:T(8,128)(2,1)}), bf16[32,64,4096]{2,1,0:T(8,128)(2,1)}, u32[]{:S(2)}, u32[]{:S(2)}) async-start(bf16[32,64,4096]{2,1,0:T(8,128)(2,1)} %stack.2), calls=%async_computation.1 | async-start | bytes 33554432 | tf_op jit(solution)/shard_map/all_to_all | solution.py:16
  387.9 6.1 copy-start.4
  387.9 26.7 %all-gather.11.cloned.1.call-start = ((), (), s32[]{:S(2)}) async-start(), calls=%async_computation.7 | async-start | bytes 6291456 | tf_op jit(solution)/shard_map/all_gather | solution.py:142
  391.9 2.1 copy-start.2
  396.2 287.6 %copy-start.18 = (f32[2048]{0:T(1024)S(1)}, f32[2048]{0:T(1024)}, u32[]{:S(2)}) copy-start(f32[2048]{0:T(1024)} %param.24) | copy-start | bytes 24580
  720.3 3.0 copy-start.5
  721.4 2.0 copy-start.3
  723.3 4.4 copy-start.12
  727.7 5.6 copy-start.1
Sparse Core Ops, SparseCore 0:
  9.0 18.8 all-gather.4
  29.6 135.3 all-gather.6
  166.6 151.4 all-gather.8
  396.4 18.2 all-gather.10
